TPU v7x, 32 devices: a whole 2x2x4 slice. The times are simulated.
32 devices in a mesh: sp: 8 (over z, y), tp: 4 (over x, core).
Axes of the slice: x: 2, y: 2, z: 4, core: 2. Of those that a mesh axis runs over, the one named last changes fastest.
Arguments:
- stream: bfloat16 [4096, 2048], P(('sp', 'tp')), may hold values from -6 to 6
- conv_value: bfloat16 [4096, 512], P('sp', 'tp'), may hold values from -6 to 6
- conv_gate: bfloat16 [4096, 512], P('sp', 'tp'), may hold values from -8 to 8
- doc_ids: int32 [4096], P('sp'), may hold values from 0 to 3, never falling along the last dimension, each value on 1 to 2048 neighbouring positions
- conv_taps: float32 [31, 512], P(None, 'tp'), may hold values from -2.2 to 2.2
- conv_bias: float32 [512], P('tp'), may hold values from -3 to 3
- chan_gain: float32 [512], replicated, may hold values from 0.1 to 1.9
- chan_shift: float32 [512], replicated, may hold values from -3 to 3
- out_weight: bfloat16 [512, 2048], replicated, may hold values from -0.25 to 0.25
- rms_gain: float32 [2048], replicated, may hold values from 0.1 to 1.9
- expert_ids: int32 [4096, 2], P(('sp', 'tp')), may hold values from 0 to 15, all different within a row; in each aligned block of 128 rows (0 to 127, 128 to 255, ...) at most 24 rows name the same one
- group_prob: float32 [4096], P(('sp', 'tp')), may hold values from 0.3 to 1
- route_logits: float32 [4096, 2], P(('sp', 'tp')), may hold values from -6 to 6
- expert_gate: bfloat16 [16, 2048, 1024], P('sp', None, 'tp'), may hold values from -0.125 to 0.125
- expert_up: bfloat16 [16, 2048, 1024], P('sp', None, 'tp'), may hold values from -0.125 to 0.125
- expert_down: bfloat16 [16, 1024, 2048], P('sp', 'tp'), may hold values from -0.1875 to 0.1875
Outputs:
- mixed: bfloat16 [4096, 2048], P(('sp', 'tp'))
Inputs may be any that keep to these rules, and one draw needn't show every extreme that they name: `expert_ids`: each row names 2 different experts. In each aligned block of 128 rows (the rows of one device) no expert is named by more than 24 rows, a bound that some block reaches. `doc_ids`: document numbers never fall along the sequence; every document has 1 to 2048 positions, one exactly 2048.
All inputs are finite; a program needn't handle non-finite values.
Results may differ from a plain program's by a relative error of at most 0.012.
Values may be sent and summed in bfloat16 or wider, within the bound.
A program may use at most 64 MiB of HBM per device.

v0:
```python
import jax
import jax.numpy as jnp
from jax import lax
from jax.sharding import PartitionSpec as P

CONV_CH = 512
eps = 1e-06


def passed_along(x, axis, by):
    size = lax.axis_size(axis)
    pairs = [(i, i + by) for i in range(size) if 0 <= i + by < size]
    return lax.ppermute(x, axis, pairs)


def causal_conv(values, gates, docs, conv_taps, conv_bias):
    reach = conv_taps.shape[0] - 1
    acts = values.astype(jnp.float32) * jax.nn.sigmoid(gates.astype(jnp.float32))
    total = values.shape[0] - reach
    result = jnp.broadcast_to(conv_bias[None, :], (total, values.shape[1]))
    own_doc = docs[reach:]
    for offset in range(reach + 1):
        begin = reach - offset
        same = (docs[begin : begin + total] == own_doc)[:, None]
        result = (
            result + jnp.where(same, acts[begin : begin + total], 0.0) * conv_taps[offset][None, :]
        )
    return result.astype(jnp.bfloat16)


def finish_norm(values, mean, square, gain, shift):
    spread = square - mean * mean
    scaled = (values - mean) * lax.rsqrt(spread + eps) * gain + shift
    return jax.nn.silu(scaled).astype(jnp.bfloat16)


def apply_experts(arrived, expert_gate, expert_up, expert_down):
    outputs = []
    for local in range(arrived.shape[1]):
        rows = arrived[:, local].reshape(-1, arrived.shape[3])
        gated = jnp.dot(rows, expert_gate[local], preferred_element_type=jnp.float32)
        upward = jnp.dot(rows, expert_up[local], preferred_element_type=jnp.float32)
        hidden = (jax.nn.silu(gated) * upward).astype(jnp.bfloat16)
        partial_value = jnp.dot(hidden, expert_down[local], preferred_element_type=jnp.float32)
        outputs.append(partial_value.reshape(arrived.shape[0], arrived.shape[2], arrived.shape[3]))
    return jnp.stack(outputs, axis=1)


def split_quarters(partial_value, quarters):
    shape = partial_value.shape
    return partial_value.astype(jnp.bfloat16).reshape(
        shape[0], shape[1], quarters, shape[2] // quarters, shape[3]
    )


def body(
    stream,
    conv_value,
    conv_gate,
    doc_ids,
    conv_taps,
    conv_bias,
    chan_gain,
    chan_shift,
    out_weight,
    rms_gain,
    expert_ids,
    group_prob,
    route_logits,
    expert_gate,
    expert_up,
    expert_down,
):
    reach = conv_taps.shape[0] - 1
    tail_value, tail_gate, tail_doc = passed_along(
        (conv_value[-reach:], conv_gate[-reach:], doc_ids[-reach:]), "sp", 1
    )
    values = jnp.concatenate([tail_value, conv_value], axis=0)
    gates = jnp.concatenate([tail_gate, conv_gate], axis=0)
    docs = jnp.concatenate([tail_doc, doc_ids], axis=0)
    conved = causal_conv(values, gates, docs, conv_taps, conv_bias)
    own_rows = stream.shape[0]
    width_local = conved.shape[1]
    lane = lax.axis_index("tp") * width_local
    floats = conved.astype(jnp.float32)
    sums, squares = lax.psum((jnp.sum(floats, axis=1), jnp.sum(floats * floats, axis=1)), "tp")
    mean = (sums / CONV_CH)[:, None]
    square = (squares / CONV_CH)[:, None]
    gain = lax.dynamic_slice_in_dim(chan_gain, lane, width_local, 0)
    shift = lax.dynamic_slice_in_dim(chan_shift, lane, width_local, 0)
    activated = finish_norm(floats, mean, square, gain, shift)
    weight_rows = lax.dynamic_slice_in_dim(out_weight, lane, width_local, 0)
    projected = lax.psum_scatter(
        jnp.dot(activated, weight_rows, preferred_element_type=jnp.float32).astype(jnp.bfloat16),
        "tp",
        scatter_dimension=0,
        tiled=True,
    ).astype(jnp.float32)
    resid = (stream.astype(jnp.float32) + projected).astype(jnp.bfloat16)
    resid_float = resid.astype(jnp.float32)
    mean_square = jnp.mean(resid_float * resid_float, axis=-1, keepdims=True)
    normed = (resid_float * lax.rsqrt(mean_square + eps) * rms_gain).astype(jnp.bfloat16)
    gap = route_logits[:, 0] - route_logits[:, 1]
    weights = jnp.stack(
        [group_prob * jax.nn.sigmoid(gap), group_prob * jax.nn.sigmoid(-gap)], axis=1
    )
    sp_count = lax.axis_size("sp")
    tp_count = lax.axis_size("tp")
    local_experts = expert_gate.shape[0]
    experts_all = sp_count * local_experts
    top_count = expert_ids.shape[1]
    capacity = max(2, 3 * own_rows * top_count // (2 * experts_all))
    flat_ids = expert_ids.reshape(-1)
    onehot = (flat_ids[:, None] == jnp.arange(experts_all, dtype=jnp.int32)[None, :]).astype(
        jnp.int32
    )
    earlier = jnp.cumsum(onehot, axis=0) - onehot
    ranks = jnp.sum(earlier * onehot, axis=1)
    dest = flat_ids * capacity + ranks
    route_token = jnp.arange(flat_ids.shape[0], dtype=jnp.int32) // top_count
    source = jnp.full((experts_all * capacity,), own_rows, jnp.int32).at[dest].set(route_token)
    with_blank = jnp.concatenate([normed, jnp.zeros((1, normed.shape[1]), jnp.bfloat16)], axis=0)
    outgoing = with_blank[source].reshape(sp_count, local_experts, capacity, normed.shape[1])
    arrived_own = lax.all_to_all(outgoing, "sp", split_axis=0, concat_axis=0, tiled=True)
    arrived = lax.all_gather(arrived_own, "tp", axis=2, tiled=True)
    partial_value = apply_experts(arrived, expert_gate, expert_up, expert_down)
    quarters = lax.all_to_all(
        split_quarters(partial_value, tp_count), "tp", split_axis=2, concat_axis=2, tiled=True
    )
    summed = jnp.sum(quarters.astype(jnp.float32), axis=2).astype(jnp.bfloat16)
    routed = lax.all_to_all(summed, "sp", split_axis=0, concat_axis=0, tiled=True)
    flat_out = routed.reshape(experts_all * capacity, normed.shape[1])
    picked = flat_out[dest].reshape(own_rows, top_count, normed.shape[1]).astype(jnp.float32)
    combined = jnp.sum(weights[:, :, None] * picked, axis=1)
    return (resid_float + combined).astype(jnp.bfloat16)


def solution(mesh):
    placed = (
        P(("sp", "tp"), None),
        P("sp", "tp"),
        P("sp", "tp"),
        P("sp"),
        P(None, "tp"),
        P("tp"),
        P(),
        P(),
        P(),
        P(),
        P(("sp", "tp"), None),
        P(("sp", "tp")),
        P(("sp", "tp"), None),
        P("sp", None, "tp"),
        P("sp", None, "tp"),
        P("sp", "tp", None),
    )
    return jax.shard_map(
        body, mesh=mesh, in_specs=placed, out_specs=P(("sp", "tp"), None), check_vma=False
    )
```

profile of v0, /device:TPU:0, one launch (start us, length us, event | category | flops | bytes accessed | tf_op | source)
XLA Modules:
  0.0 321.5 jit_solution(74922192068838987)
XLA Ops:
  6.5 0.9 slice.325
  7.4 4.9 %collective-permute-start.2 = (s32[30]{0:T(128)S(1)}, s32[30]{0:T(128)S(1)}, u32[]{:S(2)}, u32[]{:S(2)}) collective-permute-start(s32[30]{0:T(128)S(1)} %slice.325), channel_id=1, source_target_pairs={{0,4},{4,8},{8,12},{12,16},{16,20},{20,24},{24,28},{1,5},{5,9},{9,... | collective-permute-start | bytes 368 | tf_op jit(solution)/shard_map/ppermute | solution.py:13
  12.3 0.7 slice.321
  13.0 3.4 %collective-permute-start = (bf16[30,128]{1,0:T(8,128)(2,1)S(1)}, bf16[30,128]{1,0:T(8,128)(2,1)S(1)}, u32[]{:S(2)}, u32[]{:S(2)}) collective-permute-start(bf16[30,128]{1,0:T(8,128)(2,1)S(1)} %slice.321), channel_id=1, source_target_pairs={{0,4},{4,8},{8,12},{12,16},{16,20},{20,24},{24,28},{1,5},{5,9},{9,... | collective-permute-start | bytes 23048 | tf_op jit(solution)/shard_map/ppermute | solution.py:13
  16.5 0.7 slice.322
  17.2 3.4 %collective-permute-start.1 = (bf16[30,128]{1,0:T(8,128)(2,1)S(1)}, bf16[30,128]{1,0:T(8,128)(2,1)S(1)}, u32[]{:S(2)}, u32[]{:S(2)}) collective-permute-start(bf16[30,128]{1,0:T(8,128)(2,1)S(1)} %slice.322), channel_id=1, source_target_pairs={{0,4},{4,8},{8,12},{12,16},{16,20},{20,24},{24,28},{1,5},{5,9},{9,... | collective-permute-start | bytes 23048 | tf_op jit(solution)/shard_map/ppermute | solution.py:13
  20.6 1.0 slice_bitcast_fusion.30
  21.6 1.0 slice_bitcast_fusion.29
  22.6 0.8 dynamic_slice.10
  23.3 0.8 dynamic_slice.9
  24.1 0.8 pad_add_fusion
  24.8 0.8 slice_compare_fusion.29
  25.6 0.8 slice_compare_fusion.28
  26.4 1.1 divide_multiply_fusion
  27.5 3.8 %convert_reduce_fusion = (f32[512]{0:T(512)S(1)}, f32[512]{0:T(512)S(1)}, bf16[512,128]{1,0:T(8,128)(2,1)S(1)}) fusion(f32[128]{0:T(128)S(1)} %get-tuple-element.41, f32[542,128]{1,0:T(8,128)S(1)} %divide_multiply_fusion, pred[512]{0:T(512)(128)(4,1)S(1)} %get-tuple-element.71, f32[128]{0:T(128)S(1)} %get-tuple-element.42, ...), kind=kLoop, calls=%fused_computation.39 | loop fusion | flops 6355968 | bytes 8293376 | tf_op jit(solution)/shard_map/reduce_sum | solution.py:86
  31.4 5.9 %all-reduce.1 = (f32[512]{0:T(512)S(1)}, f32[512]{0:T(512)S(1)}) all-reduce(f32[512]{0:T(512)S(1)} %get-tuple-element.6, f32[512]{0:T(512)S(1)} %get-tuple-element.5), channel_id=1, replica_groups=mesh['sp'=8,'tp'=4] {'tp'}, use_global_device_ids=true, to_apply=%region_3.4 | all-reduce | flops 1024 | bytes 8192 | tf_op jit(solution)/shard_map/psum | solution.py:86
  37.3 2.1 convolution_convert_fusion.2
  39.8 0.1 eq.145
  39.9 0.6 reduce-window.6
  40.5 0.2 slice_reduce_fusion
  40.8 0.1 mul.520
  41.1 1.4 scatter_custom_fusion
  42.5 27.7 %reduce-scatter.2.cloned.1.call-done = bf16[128,2048]{1,0:T(8,128)(2,1)} async-done(((bf16[512,2048]{1,0:T(8,128)(2,1)}), bf16[128,2048]{1,0:T(8,128)(2,1)}) %reduce-scatter.2.cloned.1.call-update) | async-done | bytes 524304 | tf_op jit(solution)/shard_map/reduce_scatter | solution.py:93
  70.2 1.3 fusion.4
  71.5 1.3 fusion.6
  72.8 3.1 gather_fusion
  76.0 42.4 %all_to_all.15 = bf16[8,2,24,2048]{3,2,1,0:T(8,128)(2,1)} all-to-all(bf16[8,2,24,2048]{3,2,1,0:T(8,128)(2,1)} %bitcast.137), channel_id=1, replica_groups=mesh['sp'=8,'tp'=4] {'sp'}, dimensions={0} | all-to-all | bytes 3145728 | tf_op jit(solution)/shard_map/all_to_all | solution.py:124
  118.4 44.6 %all-gather.2.cloned.1.call-done = bf16[8,2,96,2048]{3,2,1,0:T(8,128)(2,1)} async-done(((bf16[8,2,24,2048]{3,2,1,0:T(8,128)(2,1)}), bf16[8,2,96,2048]{3,2,1,0:T(8,128)(2,1)}) %all-gather.2.cloned.1.call-update) | async-done | bytes 6291472 | tf_op jit(solution)/shard_map/all_gather | solution.py:125
  163.0 3.6 %fusion.112 = (bf16[8,1,96,2048]{3,2,1,0:T(8,128)(2,1)S(1)}, bf16[8,1,96,2048]{3,2,1,0:T(8,128)(2,1)S(1)}) fusion(bf16[8,2,96,2048]{3,2,1,0:T(8,128)(2,1)} %all-gather.2.cloned.1.call-done), kind=kLoop, calls=%fused_computation.242 | loop fusion | bytes 12582912 | tf_op jit(solution)/shard_map/slice | solution.py:40
  166.6 1.0 fusion.14
  167.6 1.0 fusion.11
  168.6 0.6 copy-done.8
  169.2 1.0 fusion.2
  170.2 1.0 fusion.3
  171.2 0.6 copy-done.9
  171.8 1.0 fusion
  172.8 1.0 fusion.1
  173.8 0.6 pad_maximum_fusion
  174.4 1.1 copy.36
  175.5 74.2 %all_to_all.16 = bf16[8,2,4,24,2048]{4,3,0,1,2:T(8,128)(2,1)} all-to-all(bf16[8,2,4,24,2048]{4,3,0,1,2:T(8,128)(2,1)S(1)} %copy.36), channel_id=1, replica_groups=mesh['sp'=8,'tp'=4] {'tp'}, dimensions={2} | all-to-all | bytes 12582912 | tf_op jit(solution)/shard_map/all_to_all | solution.py:127
  249.7 5.7 %reduce_sum.64 = bf16[8,2,24,2048]{3,2,0,1:T(8,128)(2,1)} reduce(bf16[8,2,4,24,2048]{4,3,0,1,2:T(8,128)(2,1)} %all_to_all.16, bf16[]{:T(256)} %constant.56.clone.1), dimensions={2}, to_apply=%region_10.11 | reduce | flops 2359296 | bytes 7864322 | tf_op jit(solution)/shard_map/reduce_sum | solution.py:130
  255.4 2.8 copy.38
  258.1 5.5 %all-to-all-start.2 = ((bf16[8,2,24,2048]{3,2,1,0:T(8,128)(2,1)}), bf16[8,2,24,2048]{3,2,1,0:T(8,128)(2,1)}, u32[]{:S(2)}, u32[]{:S(2)}) async-start(bf16[8,2,24,2048]{3,2,1,0:T(8,128)(2,1)} %copy.38), calls=%async_computation.3 | async-start | bytes 3145728 | tf_op jit(solution)/shard_map/all_to_all | solution.py:131
  263.8 36.6 %all-to-all-done.2 = bf16[8,2,24,2048]{3,2,1,0:T(8,128)(2,1)} async-done(((bf16[8,2,24,2048]{3,2,1,0:T(8,128)(2,1)}), bf16[8,2,24,2048]{3,2,1,0:T(8,128)(2,1)}, u32[]{:S(2)}, u32[]{:S(2)}) %all-to-all-start.2) | async-done | bytes 1572896 | tf_op jit(solution)/shard_map/all_to_all | solution.py:131
  300.4 5.0 %gather_fusion.1 = bf16[256,2048]{1,0:T(8,128)(2,1)} fusion(bf16[384,2048]{1,0:T(8,128)(2,1)} %bitcast.55, s32[1024]{0:T(1024)S(1)} %pad_clamp_fusion), kind=kCustom, calls=%fused_computation.1 | custom fusion | bytes 2098176 | tf_op jit(solution)/shard_map/gather | solution.py:133
  305.4 3.5 %reshape.150 = f32[128,2,2048]{2,1,0:T(2,128)} reshape(bf16[256,2048]{1,0:T(8,128)(2,1)} %gather_fusion.1) | data formatting | bytes 3145728 | tf_op jit(solution)/shard_map/convert_element_type | solution.py:133
  308.8 4.8 %multiply_reduce_fusion = f32[128,2048]{1,0:T(8,128)S(1)} fusion(f32[128,2,2048]{2,1,0:T(2,128)} %reshape.150, f32[128,2]{1,0:T(8,128)S(1)} %copy.31), kind=kLoop, calls=%fused_computation.9 | loop fusion | flops 786432 | bytes 3146752 | tf_op jit(solution)/shard_map/reduce_sum | solution.py:134
  313.6 1.0 fusion.7
  (44 shorter events, 0.9 us)
Async XLA Ops:
  6.5 30.7 %copy-start = (bf16[512,2048]{1,0:T(8,128)(2,1)S(1)}, bf16[512,2048]{1,0:T(8,128)(2,1)}, u32[]{:S(2)}) copy-start(bf16[512,2048]{1,0:T(8,128)(2,1)} %param.24) | copy-start | bytes 6291460
  6.5 63.7 %reduce-scatter.2.cloned.1.call-start = ((), (), s32[]{:S(2)}) async-start(), calls=%async_computation.4 | async-start | bytes 2621440 | tf_op jit(solution)/shard_map/reduce_scatter | solution.py:93
  7.4 16.6 %collective-permute-start.2 = (s32[30]{0:T(128)S(1)}, s32[30]{0:T(128)S(1)}, u32[]{:S(2)}, u32[]{:S(2)}) collective-permute-start(s32[30]{0:T(128)S(1)} %slice.325), channel_id=1, source_target_pairs={{0,4},{4,8},{8,12},{12,16},{16,20},{20,24},{24,28},{1,5},{5,9},{9,... | collective-permute-start | bytes 368 | tf_op jit(solution)/shard_map/ppermute | solution.py:13
  13.0 13.4 %collective-permute-start = (bf16[30,128]{1,0:T(8,128)(2,1)S(1)}, bf16[30,128]{1,0:T(8,128)(2,1)S(1)}, u32[]{:S(2)}, u32[]{:S(2)}) collective-permute-start(bf16[30,128]{1,0:T(8,128)(2,1)S(1)} %slice.321), channel_id=1, source_target_pairs={{0,4},{4,8},{8,12},{12,16},{16,20},{20,24},{24,28},{1,5},{5,9},{9,... | collective-permute-start | bytes 23048 | tf_op jit(solution)/shard_map/ppermute | solution.py:13
  17.2 9.2 %collective-permute-start.1 = (bf16[30,128]{1,0:T(8,128)(2,1)S(1)}, bf16[30,128]{1,0:T(8,128)(2,1)S(1)}, u32[]{:S(2)}, u32[]{:S(2)}) collective-permute-start(bf16[30,128]{1,0:T(8,128)(2,1)S(1)} %slice.322), channel_id=1, source_target_pairs={{0,4},{4,8},{8,12},{12,16},{16,20},{20,24},{24,28},{1,5},{5,9},{9,... | collective-permute-start | bytes 23048 | tf_op jit(solution)/shard_map/ppermute | solution.py:13
  31.3 8.1 %copy-start.4 = (s32[128,2]{0,1:T(2,128)S(1)}, s32[128,2]{0,1:T(2,128)}, u32[]{:S(2)}) copy-start(s32[128,2]{0,1:T(2,128)} %param.26) | copy-start | bytes 3076
  31.4 38.9 %copy-start.1 = (bf16[128,2048]{1,0:T(8,128)(2,1)S(1)}, bf16[128,2048]{1,0:T(8,128)(2,1)}, u32[]{:S(2)}) copy-start(bf16[128,2048]{1,0:T(8,128)(2,1)} %param.16) | copy-start | bytes 1572868
  37.3 34.3 %copy-start.3 = (f32[2048]{0:T(1024)S(1)}, f32[2048]{0:T(1024)}, u32[]{:S(2)}) copy-start(f32[2048]{0:T(1024)} %param.25) | copy-start | bytes 24580
  39.4 123.6 %all-gather.2.cloned.1.call-start = ((), (), s32[]{:S(2)}) async-start(), calls=%async_computation.5 | async-start | bytes 7864320 | tf_op jit(solution)/shard_map/all_gather | solution.py:125
  163.0 3.6 %copy-start.7 = (bf16[2,2048,256]{2,1,0:T(8,128)(2,1)S(1)}, bf16[2,2048,256]{2,1,0:T(8,128)(2,1)}, u32[]{:S(2)}) copy-start(bf16[2,2048,256]{2,1,0:T(8,128)(2,1)} %param.29) | copy-start | bytes 6291460
  167.6 1.6 copy-start.8
  170.2 1.6 copy-start.9
  255.4 8.3 %copy-start.5 = (f32[128,2]{0,1:T(2,128)S(1)}, f32[128,2]{0,1:T(2,128)}, u32[]{:S(2)}) copy-start(f32[128,2]{0,1:T(2,128)} %param.28) | copy-start | bytes 3076
  255.4 8.3 %copy-start.6 = (f32[128]{0:T(128)S(1)}, f32[128]{0:T(128)}, u32[]{:S(2)}) copy-start(f32[128]{0:T(128)} %param.27) | copy-start | bytes 1540
  258.1 42.3 %all-to-all-start.2 = ((bf16[8,2,24,2048]{3,2,1,0:T(8,128)(2,1)}), bf16[8,2,24,2048]{3,2,1,0:T(8,128)(2,1)}, u32[]{:S(2)}, u32[]{:S(2)}) async-start(bf16[8,2,24,2048]{3,2,1,0:T(8,128)(2,1)} %copy.38), calls=%async_computation.3 | async-start | bytes 3145728 | tf_op jit(solution)/shard_map/all_to_all | solution.py:131
  305.4 8.3 %copy-start.2 = (bf16[128,2048]{1,0:T(8,128)(2,1)S(1)}, bf16[128,2048]{1,0:T(8,128)(2,1)}, u32[]{:S(2)}) copy-start(bf16[128,2048]{1,0:T(8,128)(2,1)} %reduce-scatter.2.cloned.1.call-done) | copy-start | bytes 1572868
Sparse Core Ops, SparseCore 0:
  39.6 30.6 reduce-scatter.1
  118.6 44.4 all-gather.1
where the time goes:
time: 322 us; the launch traced here: 321 us
  blocking collectives  123 us (38%)
  waiting for transfers between devices  109 us (34%)
  local copies, waits for them, and re-layouts  28.4 us (9%)
  other arithmetic  22.6 us (7%)
  starting transfers between devices  17.3 us (5%)
  between operations  13.7 us (4%)
  matrix products  8.06 us (3%)
    all_to_all x1, blocking collectives, body(): lax.all_to_all(split_quarters(partial_value, tp_count), 'tp', split_axis=...  74.2 us
    all_gather x1, waiting for transfers between devices, body(): arrived = lax.all_gather(arrived_own, 'tp', axis=2, tiled=True)  44.6 us
    all_to_all x1, blocking collectives, body(): lax.all_to_all(outgoing, 'sp', split_axis=0, concat_axis=0, tiled=True)  42.4 us
    all_to_all x1, waiting for transfers between devices, body(): lax.all_to_all(summed, 'sp', split_axis=0, concat_axis=0, tiled=True)  36.6 us
    reduce_scatter x1, waiting for transfers between devices, body(): lax.psum_scatter(jnp.dot(activated, weight_rows, preferred_element_type=j...  27.7 us
    ppermute x3, starting transfers between devices, passed_along(): return lax.ppermute(x, axis, pairs)  11.7 us
  transfers between devices with their start and end apart: 6, of which 3 were waited for; matrix products, arithmetic and copies ran while one was open for 3% of the time, Pallas kernels for 0%

commit v1 on v0

--- a/solution.py
+++ b/solution.py
@@ -5,6 +5,14 @@
 
 CONV_CH = 512
 eps = 1e-06
+
+
+def scan_zone(x0):
+    reached = jnp.split(x0, lax.psum(1, axis_name="tp"), axis=2)
+    return jnp.concatenate(
+        lax.all_to_all(jnp.stack(reached, axis=0), axis_name="tp", split_axis=0, concat_axis=0),
+        axis=2,
+    )
 
 
 def passed_along(x, axis, by):
@@ -124,9 +132,7 @@
     arrived_own = lax.all_to_all(outgoing, "sp", split_axis=0, concat_axis=0, tiled=True)
     arrived = lax.all_gather(arrived_own, "tp", axis=2, tiled=True)
     partial_value = apply_experts(arrived, expert_gate, expert_up, expert_down)
-    quarters = lax.all_to_all(
-        split_quarters(partial_value, tp_count), "tp", split_axis=2, concat_axis=2, tiled=True
-    )
+    quarters = scan_zone(split_quarters(partial_value, tp_count))
     summed = jnp.sum(quarters.astype(jnp.float32), axis=2).astype(jnp.bfloat16)
     routed = lax.all_to_all(summed, "sp", split_axis=0, concat_axis=0, tiled=True)
     flat_out = routed.reshape(experts_all * capacity, normed.shape[1])

time: 322 us -> 322 us (level)
  no operation moved by 1% of the time
where the time goes in v1:
time: 322 us; the launch traced here: 321 us
  blocking collectives  122 us (38%)
  waiting for transfers between devices  109 us (34%)
  local copies, waits for them, and re-layouts  27.2 us (8%)
  other arithmetic  23.5 us (7%)
  starting transfers between devices  17.4 us (5%)
  between operations  13.7 us (4%)
  matrix products  8.07 us (3%)
    all_to_all x1, blocking collectives, scan_zone(): lax.all_to_all(jnp.stack(reached, axis=0), axis_name='tp', split_axis=0,...  74.2 us
    all_gather x1, waiting for transfers between devices, body(): arrived = lax.all_gather(arrived_own, 'tp', axis=2, tiled=True)  44.6 us
    all_to_all x1, blocking collectives, body(): lax.all_to_all(outgoing, 'sp', split_axis=0, concat_axis=0, tiled=True)  42.5 us
    all_to_all x1, waiting for transfers between devices, body(): lax.all_to_all(summed, 'sp', split_axis=0, concat_axis=0, tiled=True)  36.6 us
    reduce_scatter x1, waiting for transfers between devices, body(): lax.psum_scatter(jnp.dot(activated, weight_rows, preferred_element_type=j...  27.6 us
    ppermute x3, starting transfers between devices, passed_along(): return lax.ppermute(x, axis, pairs)  11.7 us
  transfers between devices with their start and end apart: 6, of which 3 were waited for; matrix products, arithmetic and copies ran while one was open for 3% of the time, Pallas kernels for 0%

profile of v1, /device:TPU:0, one launch (start us, length us, event | category | flops | bytes accessed | tf_op | source)
XLA Modules:
  0.0 321.2 jit_solution(3979163487419886621)
XLA Ops:
  6.5 0.9 slice.325
  7.4 4.9 %collective-permute-start.2 = (s32[30]{0:T(128)S(1)}, s32[30]{0:T(128)S(1)}, u32[]{:S(2)}, u32[]{:S(2)}) collective-permute-start(s32[30]{0:T(128)S(1)} %slice.325), channel_id=1, source_target_pairs={{0,4},{4,8},{8,12},{12,16},{16,20},{20,24},{24,28},{1,5},{5,9},{9,... | collective-permute-start | bytes 368 | tf_op jit(solution)/shard_map/ppermute | solution.py:21
  12.3 0.7 slice.321
  13.0 3.4 %collective-permute-start = (bf16[30,128]{1,0:T(8,128)(2,1)S(1)}, bf16[30,128]{1,0:T(8,128)(2,1)S(1)}, u32[]{:S(2)}, u32[]{:S(2)}) collective-permute-start(bf16[30,128]{1,0:T(8,128)(2,1)S(1)} %slice.321), channel_id=1, source_target_pairs={{0,4},{4,8},{8,12},{12,16},{16,20},{20,24},{24,28},{1,5},{5,9},{9,... | collective-permute-start | bytes 23048 | tf_op jit(solution)/shard_map/ppermute | solution.py:21
  16.5 0.7 slice.322
  17.2 3.4 %collective-permute-start.1 = (bf16[30,128]{1,0:T(8,128)(2,1)S(1)}, bf16[30,128]{1,0:T(8,128)(2,1)S(1)}, u32[]{:S(2)}, u32[]{:S(2)}) collective-permute-start(bf16[30,128]{1,0:T(8,128)(2,1)S(1)} %slice.322), channel_id=1, source_target_pairs={{0,4},{4,8},{8,12},{12,16},{16,20},{20,24},{24,28},{1,5},{5,9},{9,... | collective-permute-start | bytes 23048 | tf_op jit(solution)/shard_map/ppermute | solution.py:21
  20.6 1.0 slice_bitcast_fusion.30
  21.6 1.0 slice_bitcast_fusion.29
  22.6 0.8 dynamic_slice.10
  23.3 0.8 dynamic_slice.9
  24.1 0.8 pad_add_fusion
  24.8 0.8 slice_compare_fusion.29
  25.6 0.8 slice_compare_fusion.28
  26.4 1.1 divide_multiply_fusion
  27.5 3.8 %convert_reduce_fusion = (f32[512]{0:T(512)S(1)}, f32[512]{0:T(512)S(1)}, bf16[512,128]{1,0:T(8,128)(2,1)S(1)}) fusion(f32[128]{0:T(128)S(1)} %get-tuple-element.45, f32[542,128]{1,0:T(8,128)S(1)} %divide_multiply_fusion, pred[512]{0:T(512)(128)(4,1)S(1)} %get-tuple-element.75, f32[128]{0:T(128)S(1)} %get-tuple-element.46, ...), kind=kLoop, calls=%fused_computation.53 | loop fusion | flops 6355968 | bytes 8293376 | tf_op jit(solution)/shard_map/reduce_sum | solution.py:94
  31.3 5.7 %all-reduce.1 = (f32[512]{0:T(512)S(1)}, f32[512]{0:T(512)S(1)}) all-reduce(f32[512]{0:T(512)S(1)} %get-tuple-element.6, f32[512]{0:T(512)S(1)} %get-tuple-element.5), channel_id=1, replica_groups=mesh['sp'=8,'tp'=4] {'tp'}, use_global_device_ids=true, to_apply=%region_3.4 | all-reduce | flops 1024 | bytes 8192 | tf_op jit(solution)/shard_map/psum | solution.py:94
  37.1 2.1 convolution_convert_fusion.2
  39.6 0.1 eq.145
  39.8 0.6 reduce-window.6
  40.4 0.2 slice_reduce_fusion
  40.7 0.1 mul.520
  41.0 1.4 scatter_custom_fusion
  42.4 27.6 %reduce-scatter.2.cloned.1.call-done = bf16[128,2048]{1,0:T(8,128)(2,1)} async-done(((bf16[512,2048]{1,0:T(8,128)(2,1)}), bf16[128,2048]{1,0:T(8,128)(2,1)}) %reduce-scatter.2.cloned.1.call-update) | async-done | bytes 524304 | tf_op jit(solution)/shard_map/reduce_scatter | solution.py:101
  70.0 1.3 fusion.11
  71.3 1.3 fusion.13
  72.7 3.1 gather_fusion
  75.8 42.5 %all_to_all.15 = bf16[8,2,24,2048]{3,2,1,0:T(8,128)(2,1)} all-to-all(bf16[8,2,24,2048]{3,2,1,0:T(8,128)(2,1)} %bitcast.151), channel_id=1, replica_groups=mesh['sp'=8,'tp'=4] {'sp'}, dimensions={0} | all-to-all | bytes 3145728 | tf_op jit(solution)/shard_map/all_to_all | solution.py:132
  118.3 44.6 %all-gather.2.cloned.1.call-done = bf16[8,2,96,2048]{3,2,1,0:T(8,128)(2,1)} async-done(((bf16[8,2,24,2048]{3,2,1,0:T(8,128)(2,1)}), bf16[8,2,96,2048]{3,2,1,0:T(8,128)(2,1)}) %all-gather.2.cloned.1.call-update) | async-done | bytes 6291472 | tf_op jit(solution)/shard_map/all_gather | solution.py:133
  162.9 3.6 %fusion.119 = (bf16[8,1,96,2048]{3,2,1,0:T(8,128)(2,1)S(1)}, bf16[8,1,96,2048]{3,2,1,0:T(8,128)(2,1)S(1)}) fusion(bf16[8,2,96,2048]{3,2,1,0:T(8,128)(2,1)} %all-gather.2.cloned.1.call-done), kind=kLoop, calls=%fused_computation.256 | loop fusion | bytes 12582912 | tf_op jit(solution)/shard_map/slice | solution.py:48
  166.4 1.0 fusion.18
  167.5 1.0 fusion.21
  168.4 0.6 copy-done.8
  169.0 1.0 fusion.10
  170.0 1.0 fusion.9
  171.0 0.6 copy-done.9
  171.6 1.0 fusion.1
  172.6 1.0 fusion
  173.6 0.6 fusion.5
  174.2 0.8 pad_maximum_fusion
  175.1 74.2 %all_to_all.16 = bf16[4,8,2,1,24,2048]{5,4,1,2,3,0:T(8,128)(2,1)} all-to-all(bf16[4,8,2,1,24,2048]{5,4,1,2,3,0:T(8,128)(2,1)S(1)} %pad_maximum_fusion), channel_id=1, replica_groups=mesh['sp'=8,'tp'=4] {'tp'}, dimensions={0} | all-to-all | bytes 12582912 | tf_op jit(solution)/shard_map/all_to_all | solution.py:13
  249.3 5.7 %reduce_sum.64 = bf16[8,2,24,2048]{3,2,0,1:T(8,128)(2,1)} reduce(bf16[4,8,2,1,24,2048]{5,4,1,2,3,0:T(8,128)(2,1)} %all_to_all.16, bf16[]{:T(256)} %constant.56.clone.1), dimensions={0,3}, to_apply=%region_10.11 | reduce | flops 2359296 | bytes 7864322 | tf_op jit(solution)/shard_map/reduce_sum | solution.py:136
  255.0 2.7 copy.46
  257.7 5.6 %all-to-all-start.2 = ((bf16[8,2,24,2048]{3,2,1,0:T(8,128)(2,1)}), bf16[8,2,24,2048]{3,2,1,0:T(8,128)(2,1)}, u32[]{:S(2)}, u32[]{:S(2)}) async-start(bf16[8,2,24,2048]{3,2,1,0:T(8,128)(2,1)} %copy.46), calls=%async_computation.3 | async-start | bytes 3145728 | tf_op jit(solution)/shard_map/all_to_all | solution.py:137
  263.5 36.6 %all-to-all-done.2 = bf16[8,2,24,2048]{3,2,1,0:T(8,128)(2,1)} async-done(((bf16[8,2,24,2048]{3,2,1,0:T(8,128)(2,1)}), bf16[8,2,24,2048]{3,2,1,0:T(8,128)(2,1)}, u32[]{:S(2)}, u32[]{:S(2)}) %all-to-all-start.2) | async-done | bytes 1572896 | tf_op jit(solution)/shard_map/all_to_all | solution.py:137
  300.1 5.0 %gather_fusion.1 = bf16[256,2048]{1,0:T(8,128)(2,1)} fusion(bf16[384,2048]{1,0:T(8,128)(2,1)} %bitcast.59, s32[1024]{0:T(1024)S(1)} %pad_clamp_fusion), kind=kCustom, calls=%fused_computation.1 | custom fusion | bytes 2098176 | tf_op jit(solution)/shard_map/gather | solution.py:139
  305.1 3.4 %reshape.152 = f32[128,2,2048]{2,1,0:T(2,128)} reshape(bf16[256,2048]{1,0:T(8,128)(2,1)} %gather_fusion.1) | data formatting | bytes 3145728 | tf_op jit(solution)/shard_map/convert_element_type | solution.py:139
  308.5 4.9 %multiply_reduce_fusion = f32[128,2048]{1,0:T(8,128)S(1)} fusion(f32[128,2,2048]{2,1,0:T(2,128)} %reshape.152, f32[128,2]{1,0:T(8,128)S(1)} %copy.38), kind=kLoop, calls=%fused_computation.15 | loop fusion | flops 786432 | bytes 3146752 | tf_op jit(solution)/shard_map/reduce_sum | solution.py:140
  313.3 1.0 fusion.14
  (44 shorter events, 0.9 us)
Async XLA Ops:
  6.5 30.6 %copy-start = (bf16[512,2048]{1,0:T(8,128)(2,1)S(1)}, bf16[512,2048]{1,0:T(8,128)(2,1)}, u32[]{:S(2)}) copy-start(bf16[512,2048]{1,0:T(8,128)(2,1)} %param.24) | copy-start | bytes 6291460
  6.5 63.5 %reduce-scatter.2.cloned.1.call-start = ((), (), s32[]{:S(2)}) async-start(), calls=%async_computation.4 | async-start | bytes 2621440 | tf_op jit(solution)/shard_map/reduce_scatter | solution.py:101
  7.4 16.6 %collective-permute-start.2 = (s32[30]{0:T(128)S(1)}, s32[30]{0:T(128)S(1)}, u32[]{:S(2)}, u32[]{:S(2)}) collective-permute-start(s32[30]{0:T(128)S(1)} %slice.325), channel_id=1, source_target_pairs={{0,4},{4,8},{8,12},{12,16},{16,20},{20,24},{24,28},{1,5},{5,9},{9,... | collective-permute-start | bytes 368 | tf_op jit(solution)/shard_map/ppermute | solution.py:21
  13.0 13.4 %collective-permute-start = (bf16[30,128]{1,0:T(8,128)(2,1)S(1)}, bf16[30,128]{1,0:T(8,128)(2,1)S(1)}, u32[]{:S(2)}, u32[]{:S(2)}) collective-permute-start(bf16[30,128]{1,0:T(8,128)(2,1)S(1)} %slice.321), channel_id=1, source_target_pairs={{0,4},{4,8},{8,12},{12,16},{16,20},{20,24},{24,28},{1,5},{5,9},{9,... | collective-permute-start | bytes 23048 | tf_op jit(solution)/shard_map/ppermute | solution.py:21
  17.2 9.2 %collective-permute-start.1 = (bf16[30,128]{1,0:T(8,128)(2,1)S(1)}, bf16[30,128]{1,0:T(8,128)(2,1)S(1)}, u32[]{:S(2)}, u32[]{:S(2)}) collective-permute-start(bf16[30,128]{1,0:T(8,128)(2,1)S(1)} %slice.322), channel_id=1, source_target_pairs={{0,4},{4,8},{8,12},{12,16},{16,20},{20,24},{24,28},{1,5},{5,9},{9,... | collective-permute-start | bytes 23048 | tf_op jit(solution)/shard_map/ppermute | solution.py:21
  37.1 2.2 copy-start.4
  37.1 32.9 %copy-start.1 = (bf16[128,2048]{1,0:T(8,128)(2,1)S(1)}, bf16[128,2048]{1,0:T(8,128)(2,1)}, u32[]{:S(2)}) copy-start(bf16[128,2048]{1,0:T(8,128)(2,1)} %param.16) | copy-start | bytes 1572868
  39.3 32.1 %copy-start.3 = (f32[2048]{0:T(1024)S(1)}, f32[2048]{0:T(1024)}, u32[]{:S(2)}) copy-start(f32[2048]{0:T(1024)} %param.25) | copy-start | bytes 24580
  39.3 123.6 %all-gather.2.cloned.1.call-start = ((), (), s32[]{:S(2)}) async-start(), calls=%async_computation.5 | async-start | bytes 7864320 | tf_op jit(solution)/shard_map/all_gather | solution.py:133
  162.9 3.6 %copy-start.7 = (bf16[2,2048,256]{2,1,0:T(8,128)(2,1)S(1)}, bf16[2,2048,256]{2,1,0:T(8,128)(2,1)}, u32[]{:S(2)}) copy-start(bf16[2,2048,256]{2,1,0:T(8,128)(2,1)} %param.29) | copy-start | bytes 6291460
  167.4 1.6 copy-start.8
  170.0 1.6 copy-start.9
  257.7 5.7 %copy-start.5 = (f32[128,2]{0,1:T(2,128)S(1)}, f32[128,2]{0,1:T(2,128)}, u32[]{:S(2)}) copy-start(f32[128,2]{0,1:T(2,128)} %param.28) | copy-start | bytes 3076
  257.7 5.7 %copy-start.6 = (f32[128]{0:T(128)S(1)}, f32[128]{0:T(128)}, u32[]{:S(2)}) copy-start(f32[128]{0:T(128)} %param.27) | copy-start | bytes 1540
  257.7 42.4 %all-to-all-start.2 = ((bf16[8,2,24,2048]{3,2,1,0:T(8,128)(2,1)}), bf16[8,2,24,2048]{3,2,1,0:T(8,128)(2,1)}, u32[]{:S(2)}, u32[]{:S(2)}) async-start(bf16[8,2,24,2048]{3,2,1,0:T(8,128)(2,1)} %copy.46), calls=%async_computation.3 | async-start | bytes 3145728 | tf_op jit(solution)/shard_map/all_to_all | solution.py:137
  308.5 4.9 %copy-start.2 = (bf16[128,2048]{1,0:T(8,128)(2,1)S(1)}, bf16[128,2048]{1,0:T(8,128)(2,1)}, u32[]{:S(2)}) copy-start(bf16[128,2048]{1,0:T(8,128)(2,1)} %reduce-scatter.2.cloned.1.call-done) | copy-start | bytes 1572868
Sparse Core Ops, SparseCore 0:
  39.4 30.5 reduce-scatter.1
  118.4 44.4 all-gather.1
